TPU v7x, 128 devices: a whole 4x4x4 slice. The times are simulated.
128 devices in a mesh: sp: 16 (over z, y), tp: 8 (over x, core).
Axes of the slice: x: 4, y: 4, z: 4, core: 2. Of those that a mesh axis runs over, the one named last changes fastest.
Arguments:
- resid: bfloat16 [16384, 2048], P(('sp', 'tp')), may hold values from -6 to 6
- query_nope: bfloat16 [16384, 2048], P('sp', 'tp'), may hold values from -18 to 18
- query_rope: bfloat16 [16384, 1024], P('sp', 'tp'), may hold values from -300 to 300
- latent: bfloat16 [16384, 256], P('sp'), may hold values from -6 to 6
- key_rope: bfloat16 [16384, 64], P('sp'), may hold values from -6 to 6
- latent_gain: float32 [256], replicated, may hold values from 0.1 to 1.9
- w_key: bfloat16 [256, 2048], P(None, 'tp'), may hold values from -0.375 to 0.375
- w_value: bfloat16 [256, 2048], P(None, 'tp'), may hold values from -0.375 to 0.375
- w_out: bfloat16 [2048, 2048], P('tp'), may hold values from -0.125 to 0.125
- mix_gain: float32 [2048], replicated, may hold values from 0.1 to 1.9
- w_gate: bfloat16 [2048, 5632], P('sp', 'tp'), may hold values from -0.125 to 0.125
- w_up: bfloat16 [2048, 5632], P('sp', 'tp'), may hold values from -0.125 to 0.125
- w_down: bfloat16 [2048, 5632], P('sp', 'tp'), may hold values from -0.078125 to 0.078125
Outputs:
- layer_out: bfloat16 [16384, 2048], P(('sp', 'tp'))
All inputs are finite; a program needn't handle non-finite values.
Results may differ from a plain program's by a relative error of at most 0.0095.
Values may be sent and summed in bfloat16 or wider, within the bound.
No kernel may reach another device: no remote copies, remote signals or barrier semaphores. Data moves between devices by JAX's collectives and lax.ppermute only.
A program may use at most 128 MiB of HBM per device.

v0:
```python
import jax
import jax.numpy as jnp
from jax import lax
from jax.sharding import PartitionSpec as P

NOPE = 128
ROPE = 64
VDIM = 128
norm_eps = 1e-06
masked_score = -1e30
theta_base = 10000.0


def in_one_piece(arrays, axis, dim, along):
    both = jnp.concatenate(arrays, axis=along)
    filled, at, gathered = (lax.all_gather(both, axis, axis=dim, tiled=True), 0, [])
    for a in arrays:
        gathered.append(lax.slice_in_dim(filled, at, at + a.shape[along], axis=along))
        at += a.shape[along]
    return tuple(gathered)


def split_up(array, dim, count):
    lengths = array.shape
    tiles = array.reshape(*lengths[:dim], count, lengths[dim] // count, *lengths[dim + 1 :])
    return jnp.moveaxis(tiles, dim, 0)


def summed_on_arrival(array, axis, dim):
    tiles = split_up(array, dim, lax.axis_size(axis))
    arrived = lax.all_to_all(tiles, axis, split_axis=0, concat_axis=0, tiled=True)
    return arrived.astype(jnp.float32).sum(axis=0)


def rotate(values_in, angle):
    half_width = values_in.shape[-1] // 2
    front_half = values_in[..., :half_width]
    back_half = values_in[..., half_width:]
    cosine = jnp.cos(angle)
    sine_part = jnp.sin(angle)
    return jnp.concatenate(
        [front_half * cosine - back_half * sine_part, back_half * cosine + front_half * sine_part],
        axis=-1,
    )


def angles(positions, full_width):
    half_width = full_width // 2
    frequency = theta_base ** (-2.0 * jnp.arange(half_width).astype(jnp.float32) / full_width)
    return positions[:, None] * frequency[None, :]


def rms_scale(values_in, gain):
    return (
        values_in
        * lax.rsqrt(jnp.mean(values_in * values_in, axis=-1, keepdims=True) + norm_eps)
        * gain
    )


def attend(fold_state, queries, key_block, value_block, rope_block, block_start):
    nope_query, rope_query, query_rows = queries
    running_max, weight_sum, accumulated = fold_state
    key_rows = block_start + jnp.arange(key_block.shape[0], dtype=jnp.int32)
    causal = key_rows[None, :] <= query_rows[:, None]
    scores = jnp.einsum("qhd,khd->hqk", nope_query, key_block, preferred_element_type=jnp.float32)
    scores = scores + jnp.einsum(
        "qhr,kr->hqk", rope_query, rope_block, preferred_element_type=jnp.float32
    )
    scores = jnp.where(causal[None], scores * (NOPE + ROPE) ** (-0.5), masked_score)
    new_max = jnp.maximum(running_max, jnp.max(scores, axis=-1))
    weights = jnp.where(causal[None], jnp.exp(scores - new_max[..., None]), 0.0)
    factor = jnp.exp(running_max - new_max)
    weight_sum = weight_sum * factor + jnp.sum(weights, axis=-1)
    accumulated = accumulated * factor[..., None] + jnp.einsum(
        "hqk,khd->hqd",
        weights.astype(jnp.bfloat16),
        value_block,
        preferred_element_type=jnp.float32,
    )
    return (new_max, weight_sum, accumulated)


def over_blocks(fold_state, arrays, last_query, step_fn, row_count):
    piece_rows = arrays[0].shape[0]
    candidates = [
        row_count * multiple
        for multiple in (4, 2, 1)
        if piece_rows % (row_count * multiple) == 0 and row_count * multiple <= 2048
    ]
    block_rows = candidates[0]
    block_count = piece_rows // block_rows
    stacked = tuple(
        (member.reshape((block_count, block_rows) + member.shape[1:]) for member in arrays)
    )

    def advance(state_in, indexed):
        block_index, blocks_now = indexed
        block_start = block_index * block_rows

        def compute(state_now):
            return step_fn(state_now, blocks_now, block_start)

        def unchanged(state_now):
            return state_now

        return (lax.cond(block_start <= last_query, compute, unchanged, state_in), None)

    result, ignored = lax.scan(
        advance, fold_state, (jnp.arange(block_count, dtype=jnp.int32), stacked)
    )
    return result


def on_device(
    resid,
    query_nope,
    query_rope,
    latent,
    key_rope,
    latent_gain,
    w_key,
    w_value,
    w_out,
    mix_gain,
    w_gate,
    w_up,
    w_down,
):
    row_count = query_nope.shape[0]
    head_count = query_nope.shape[1] // NOPE
    first_row = lax.axis_index("sp") * row_count
    query_rows = first_row + jnp.arange(row_count, dtype=jnp.int32)
    angle = angles(query_rows.astype(jnp.float32), ROPE)
    nope_query = query_nope.reshape(row_count, head_count, NOPE)
    rope_query = rotate(
        query_rope.astype(jnp.float32).reshape(row_count, head_count, ROPE), angle[:, None, :]
    ).astype(jnp.bfloat16)
    latent_normed = rms_scale(latent.astype(jnp.float32), latent_gain).astype(jnp.bfloat16)
    key_rotated = rotate(key_rope.astype(jnp.float32), angle).astype(jnp.bfloat16)
    queries = (nope_query, rope_query, query_rows)
    last_query = first_row + row_count - 1
    initial = (
        jnp.full((head_count, row_count), masked_score, jnp.float32),
        jnp.zeros((head_count, row_count), jnp.float32),
        jnp.zeros((head_count, row_count, VDIM), jnp.float32),
    )
    gate_full, up_full, down_full = in_one_piece((w_gate, w_up, w_down), "sp", 0, 1)

    def expand_block(state_now, blocks_now, block_start):
        latent_block, rope_block = blocks_now
        key_block = jnp.dot(latent_block, w_key, preferred_element_type=jnp.float32).astype(
            jnp.bfloat16
        )
        value_block = jnp.dot(latent_block, w_value, preferred_element_type=jnp.float32).astype(
            jnp.bfloat16
        )
        return attend(
            state_now,
            queries,
            key_block.reshape(-1, head_count, NOPE),
            value_block.reshape(-1, head_count, VDIM),
            rope_block,
            block_start,
        )

    final_state = over_blocks(
        initial,
        in_one_piece((latent_normed, key_rotated), "sp", 0, 1),
        last_query,
        expand_block,
        row_count,
    )
    head_out = (final_state[2] / final_state[1][..., None]).astype(jnp.bfloat16)
    out_heads = w_out.reshape(head_count, VDIM, w_out.shape[1])
    part_rows = head_out
    head_term = jnp.einsum("hqv,hvd->qd", part_rows, out_heads, preferred_element_type=jnp.float32)
    attention_proj = summed_on_arrival(
        lax.optimization_barrier(head_term.astype(jnp.bfloat16))
        .astype(jnp.float32)
        .astype(jnp.bfloat16),
        "tp",
        0,
    )
    stream = resid.astype(jnp.float32) + attention_proj
    normed = rms_scale(stream, mix_gain).astype(jnp.bfloat16)
    row_piece = lax.all_gather(normed, "tp", axis=0, tiled=True)
    gate_value = jnp.dot(row_piece, gate_full, preferred_element_type=jnp.float32)
    upward = jnp.dot(row_piece, up_full, preferred_element_type=jnp.float32)
    hidden = (jax.nn.silu(gate_value) * upward).astype(jnp.bfloat16)
    part_rows = hidden
    down_term = lax.dot_general(
        part_rows, down_full, (((1,), (1,)), ((), ())), preferred_element_type=jnp.float32
    )
    mixer_out = lax.psum_scatter(
        lax.optimization_barrier(down_term.astype(jnp.bfloat16))
        .astype(jnp.float32)
        .astype(jnp.bfloat16),
        "tp",
        scatter_dimension=0,
        tiled=True,
    ).astype(jnp.float32)
    return (stream + 0.5 * mixer_out).astype(jnp.bfloat16)


def solution(mesh):
    return jax.shard_map(
        on_device,
        mesh=mesh,
        in_specs=(
            P(("sp", "tp"), None),
            P("sp", "tp"),
            P("sp", "tp"),
            P("sp", None),
            P("sp", None),
            P(),
            P(None, "tp"),
            P(None, "tp"),
            P("tp", None),
            P(),
            P("sp", "tp"),
            P("sp", "tp"),
            P("sp", "tp"),
        ),
        out_specs=P(("sp", "tp"), None),
        check_vma=False,
    )
```

profile of v0, /device:TPU:0, one launch (start us, length us, event | category | flops | bytes accessed | tf_op | source)
XLA Modules:
  0.0 639.9 jit_solution(16293472215441492424)
XLA Ops:
  8.6 1.3 fusion.31
  9.9 1.2 fusion.33
  11.2 1.1 pad_maximum_fusion
  14.7 90.1 %all-gather.4.cloned.1.call-done = bf16[16384,320]{1,0:T(8,128)(2,1)} async-done(((bf16[1024,320]{1,0:T(8,128)(2,1)}), bf16[16384,320]{1,0:T(8,128)(2,1)}) %all-gather.4.cloned.1.call-update) | async-done | bytes 10485776 | tf_op jit(solution)/shard_map/all_gather | solution.py:16
  104.9 3.7 slice.39
  108.5 4.8 copy.29
  113.3 7.1 %slice.38 = bf16[16384,256]{1,0:T(8,128)(2,1)} slice(bf16[16384,320]{1,0:T(8,128)(2,1)} %all-gather.4.cloned.1.call-done), slice={[0:16384], [0:256]} | slice | bytes 16777216 | tf_op jit(solution)/shard_map/slice | solution.py:18
  122.7 59.4 %while.15 = (s32[]{:T(128)}, f32[2,1024]{1,0:T(2,128)S(1)}, f32[2,1024]{1,0:T(2,128)}, f32[2,1024,128]{2,1,0:T(8,128)}, s32[8]{0:T(128)}, /*index=5*/s32[]{:T(12...) while((s32[]{:T(128)}, f32[2,1024]{1,0:T(2,128)S(1)}, ...), condition=%wide.region_6.7_spmd.clone, body=%wide.region_1.6_spmd.clone.sunk | while | flops 3266845696 | bytes 178161584 | solution.py:109
  122.7 1.3 dynamic_slice.38
  124.6 43.7 %conditional.3 = ((f32[2,1024]{1,0:T(2,128)S(1)}, f32[2,1024]{1,0:T(2,128)}, f32[2,1024,128]{2,1,0:T(8,128)})) conditional(s32[]{:T(128)} %convert_element_type.126, (f32[2,1024]{1,0:T(2,128)S(1)}, f32[2,1024]{1,0:T(2,128)}, f32[2,1024,128]{2,1,0:T(8,128)}) %tuple.44, (s32[]{:T(128)}, s32[]{:T(128)}, bf16[8,2048,256]{2,1,0:T(8,128)(2,1)}, s32[]{:T(128)}, ...), branch_computations={%region_2.2_spmd, %region_3.5_spmd} | conditional | flops 3266845696 | bytes 178157184 | solution.py:107
  124.6 1.8 convolution_convert_fusion.1
  126.4 8.1 %fusion.37 = f32[2,2048,1024]{2,1,0:T(8,128)} fusion(bf16[2048,2,128]{0,2,1:T(8,128)(2,1)S(1)} %bitcast.42, bf16[1024,2,128]{2,0,1:T(8,128)(2,1)S(1)} %get-tuple-element.152), kind=kOutput, calls=%fused_computation.62 | convolution fusion | flops 1073741824 | bytes 18350080 | tf_op jit(solution)/shard_map/while/body/eval_jaxpr/cond/branch_1_fun/qhd,khd->hqk/dot_general | solution.py:66
  134.5 1.3 broadcast_compare_fusion
  135.9 12.3 %fusion.36 = (f32[2,1024]{1,0:T(2,128)S(1)}, f32[2,1024,2048]{1,2,0:T(8,128)}) fusion(bf16[1024,2,64]{0,2,1:T(8,128)(2,1)} %get-tuple-element.154, bf16[8,2048,64]{1,2,0:T(8,128)(2,1)} %get-tuple-element.153, s32[]{:T(128)} %get-tuple-element.150, f32[2,2048,1024]{2,1,0:T(8,128)} %fusion.37, pred[1024,2048]{0,1:T(8,128)(4,1)S(1)} %broadcast_compare_fusion), kind=kOutput, calls=%fused_computation.61 | convolution fusion | flops 553646080 | bytes 36184576 | tf_op jit(solution)/shard_map/while/body/eval_jaxpr/cond/branch_1_fun/qhr,kr->hqk/dot_general | solution.py:67
  148.2 8.6 %fusion.5 = f32[2,1024]{1,0:T(2,128)S(1)} fusion(f32[2,1024,2048]{1,2,0:T(8,128)} %get-tuple-element.256, f32[2,1024]{1,0:T(2,128)S(1)} %max.4, pred[1024,2048]{0,1:T(8,128)(4,1)} %copy-done.2), kind=kLoop, calls=%fused_computation.6 | loop fusion | flops 12580864 | bytes 18890752 | tf_op jit(solution)/shard_map/while/body/eval_jaxpr/cond/branch_1_fun/reduce_sum | solution.py:74
  156.8 2.1 multiply_add_fusion
  158.9 1.8 convolution_convert_fusion
  160.6 7.7 %fusion.9 = f32[2,1024,128]{2,1,0:T(8,128)} fusion(bf16[2048,2,128]{0,2,1:T(8,128)(2,1)S(1)} %bitcast.44, f32[2,1024,2048]{1,2,0:T(8,128)S(1)} %copy-done.1, f32[2,1024]{1,0:T(2,128)S(1)} %max.4, pred[1024,2048]{0,1:T(8,128)(4,1)} %copy-done.2, f32[2,1024,128]{2,1,0:T(8,128)} %get-tuple-element.156, f32[2,1024]{1,0:T(2,128)S(1)} %get-tuple-element.254), kind=kOutput, calls=%fused_computation.12 | convolution fusion | flops 1086849024 | bytes 22036480 | tf_op jit(solution)/shard_map/while/body/eval_jaxpr/cond/branch_1_fun/hqk,khd->hqd/dot_general | solution.py:75
  168.3 1.3 dynamic_slice.38
  170.3 1.3 dynamic_slice.38
  172.2 1.3 dynamic_slice.38
  174.2 1.3 dynamic_slice.38
  176.2 1.3 dynamic_slice.38
  178.1 1.3 dynamic_slice.38
  180.1 1.3 dynamic_slice.38
  182.1 2.5 bitcast_convert_fusion
  184.6 53.7 %all_to_all.5 = bf16[8,128,2048]{2,1,0:T(8,128)(2,1)S(1)} all-to-all(bf16[8,128,2048]{2,1,0:T(8,128)(2,1)S(1)} %bitcast.46), channel_id=1, replica_groups=mesh['sp'=16,'tp'=8] {'tp'}, dimensions={0} | all-to-all | bytes 8388608 | tf_op jit(solution)/shard_map/all_to_all | solution.py:31
  240.7 332.6 %all-gather.6.cloned.1.call-done = bf16[1024,2048]{1,0:T(8,128)(2,1)} async-done(((bf16[128,2048]{1,0:T(8,128)(2,1)}), bf16[1024,2048]{1,0:T(8,128)(2,1)}) %all-gather.6.cloned.1.call-update) | async-done | bytes 4194320 | tf_op jit(solution)/shard_map/all_gather | solution.py:187
  573.4 7.9 %fusion.25 = f32[1024,704]{0,1:T(8,128)} fusion(bf16[1024,2048]{1,0:T(8,128)(2,1)} %all-gather.6.cloned.1.call-done, bf16[2048,2112]{0,1:T(8,128)(2,1)} %all-gather.8.cloned.1.call-done), kind=kOutput, calls=%fused_computation.33 | convolution fusion | flops 2952790016 | bytes 9961472 | tf_op jit(solution)/shard_map/dot_general | solution.py:188
  581.3 12.0 %convolution_convert_fusion.2 = bf16[1024,2048]{1,0:T(8,128)(2,1)} fusion(bf16[2048,2112]{0,1:T(8,128)(2,1)} %all-gather.8.cloned.1.call-done, f32[1024,704]{0,1:T(8,128)} %fusion.25, bf16[1024,2048]{1,0:T(8,128)(2,1)} %all-gather.6.cloned.1.call-done), kind=kOutput, calls=%fused_computation.29 | convolution fusion | flops 5912002560 | bytes 17039360 | tf_op jit(solution)/shard_map/dot_general | solution.py:192
  593.3 38.0 %reduce-scatter.2.cloned.1.call-done = bf16[128,2048]{1,0:T(8,128)(2,1)} async-done(((bf16[1024,2048]{1,0:T(8,128)(2,1)}), bf16[128,2048]{1,0:T(8,128)(2,1)}) %reduce-scatter.2.cloned.1.call-update) | async-done | bytes 524304 | tf_op jit(solution)/shard_map/reduce_scatter | solution.py:195
  631.3 2.0 add_convert_fusion
  (71 shorter events, 9.1 us)
Async XLA Ops:
  6.5 175.5 %copy-start = (bf16[256,2048]{1,0:T(8,128)(2,1)S(1)}, bf16[256,2048]{1,0:T(8,128)(2,1)}, u32[]{:S(2)}) copy-start(bf16[256,2048]{1,0:T(8,128)(2,1)} %param.25) | copy-start | bytes 3145732
  6.5 5.8 copy-start.9
  6.5 5.8 copy-start.8
  6.5 5.8 copy-start.7
  6.5 6.7 %copy-start.6 = (bf16[1024,128]{1,0:T(8,128)(2,1)S(1)}, bf16[1024,128]{1,0:T(8,128)(2,1)}, u32[]{:S(2)}) copy-start(bf16[1024,128]{1,0:T(8,128)(2,1)} %param.19) | copy-start | bytes 786436
  6.5 6.9 %copy-start.5 = (bf16[1024,256]{1,0:T(8,128)(2,1)S(1)}, bf16[1024,256]{1,0:T(8,128)(2,1)}, u32[]{:S(2)}) copy-start(bf16[1024,256]{1,0:T(8,128)(2,1)} %param.18) | copy-start | bytes 1572868
  6.6 98.3 %all-gather.4.cloned.1.call-start = ((), (), s32[]{:S(2)}) async-start(), calls=%async_computation.2 | async-start | bytes 13369344 | tf_op jit(solution)/shard_map/all_gather | solution.py:16
  12.3 228.4 %all-gather.8.cloned.1.call-start = ((), (), s32[]{:S(2)}) async-start(), calls=%async_computation.4 | async-start | bytes 9191424 | tf_op jit(solution)/shard_map/all_gather | solution.py:16
  13.2 560.1 %all-gather.6.cloned.1.call-start = ((), (), s32[]{:S(2)}) async-start(), calls=%async_computation.3 | async-start | bytes 4718592 | tf_op jit(solution)/shard_map/all_gather | solution.py:187
  135.9 12.3 %copy-start.2 = (pred[1024,2048]{0,1:T(8,128)(4,1)}, pred[1024,2048]{0,1:T(8,128)(4,1)S(1)}, u32[]{:S(2)}) copy-start(pred[1024,2048]{0,1:T(8,128)(4,1)S(1)} %broadcast_compare_fusion) | copy-start | bytes 6291460 | tf_op jit(solution)/shard_map/while/body/eval_jaxpr/cond
  148.2 10.7 %copy-start.4 = (bf16[256,256]{1,0:T(8,128)(2,1)S(1)}, bf16[256,256]{1,0:T(8,128)(2,1)}, u32[]{:S(2)}) copy-start(bf16[256,256]{1,0:T(8,128)(2,1)} %get-tuple-element.157) | copy-start | bytes 393220 | tf_op jit(solution)/shard_map/while/body/eval_jaxpr/cond
  148.2 12.5 %copy-start.1 = (f32[2,1024,2048]{1,2,0:T(8,128)S(1)}, f32[2,1024,2048]{1,2,0:T(8,128)}, u32[]{:S(2)}) copy-start(f32[2,1024,2048]{1,2,0:T(8,128)} %get-tuple-element.256) | copy-start | bytes 50331652 | tf_op jit(solution)/shard_map/while/body/eval_jaxpr/cond
  238.4 1.0 copy-start.3
  238.4 1.3 copy-start.10
  240.6 390.7 %reduce-scatter.2.cloned.1.call-start = ((), (), s32[]{:S(2)}) async-start(), calls=%async_computation.5 | async-start | bytes 4718592 | tf_op jit(solution)/shard_map/reduce_scatter | solution.py:195
Sparse Core Ops, SparseCore 0:
  12.4 92.3 all-gather.3
  107.0 78.2 all-gather.7
  240.7 332.5 all-gather.5
  593.4 37.8 reduce-scatter.1
where the time goes:
time: 641 us; the launch traced here: 640 us
  waiting for transfers between devices  461 us (72%)
  matrix products  54 us (8%)
  blocking collectives  53.7 us (8%)
  local copies, waits for them, and re-layouts  29.4 us (5%)
  other arithmetic  22.9 us (4%)
  between operations  13.3 us (2%)
    all_gather x1, waiting for transfers between devices, on_device(): row_piece = lax.all_gather(normed, 'tp', axis=0, tiled=True)  333 us
    all_gather x2, waiting for transfers between devices, in_one_piece(): lax.all_gather(both, axis, axis=dim, tiled=True)  90.1 us
    all_to_all x1, blocking collectives, summed_on_arrival(): lax.all_to_all(tiles, axis, split_axis=0, concat_axis=0, tiled=True)  53.7 us
    reduce_scatter x1, waiting for transfers between devices, on_device(): lax.psum_scatter(lax.optimization_barrier(down_term.astype(jnp.bfloat16))...  38 us
  transfers between devices with their start and end apart: 4, of which 3 were waited for; matrix products, arithmetic and copies ran while one was open for 12% of the time, Pallas kernels for 0%

commit v1 on v0

--- a/solution.py
+++ b/solution.py
@@ -184,7 +184,14 @@
     )
     stream = resid.astype(jnp.float32) + attention_proj
     normed = rms_scale(stream, mix_gain).astype(jnp.bfloat16)
-    row_piece = lax.all_gather(normed, "tp", axis=0, tiled=True)
+
+    def sites_work(obj, mesh_ax, ndim_at):
+        v1 = tuple((obj for _ in range(jax.lax.psum(1, mesh_ax))))
+        found_now = jnp.stack(v1)
+        d_next = jax.lax.all_to_all(found_now, mesh_ax, 0, 0)
+        return jnp.concatenate(d_next, axis=ndim_at)
+
+    row_piece = sites_work(normed, "tp", 0)
     gate_value = jnp.dot(row_piece, gate_full, preferred_element_type=jnp.float32)
     upward = jnp.dot(row_piece, up_full, preferred_element_type=jnp.float32)
     hidden = (jax.nn.silu(gate_value) * upward).astype(jnp.bfloat16)

time: 641 us -> 663 us (1.034)
  waiting for transfers between devices: 461 us -> 479 us
    all_gather x1 -> x0, waiting for transfers between devices: 333 us -> none  [on_device(): row_piece = lax.all_gather(normed, 'tp', axis=0, tiled=True)]
    reduce_scatter x1, waiting for transfers between devices: 38 us -> 339 us  [on_device(): lax.psum_scatter(lax.optimization_barrier(down_term.astype(jnp.bfloat16))...]
    all_to_all x0 -> x1, waiting for transfers between devices: none -> 49.6 us  [sites_work(): d_next = jax.lax.all_to_all(found_now, mesh_ax, 0, 0)]
where the time goes in v1:
time: 663 us; the launch traced here: 662 us
  waiting for transfers between devices  479 us (72%)
  matrix products  54.1 us (8%)
  blocking collectives  53.7 us (8%)
  local copies, waits for them, and re-layouts  30.8 us (5%)
  other arithmetic  22 us (3%)
  between operations  13.3 us (2%)
    reduce_scatter x1, waiting for transfers between devices, on_device(): lax.psum_scatter(lax.optimization_barrier(down_term.astype(jnp.bfloat16))...  339 us
    all_gather x2, waiting for transfers between devices, in_one_piece(): lax.all_gather(both, axis, axis=dim, tiled=True)  90.2 us
    all_to_all x1, blocking collectives, summed_on_arrival(): lax.all_to_all(tiles, axis, split_axis=0, concat_axis=0, tiled=True)  53.7 us
    all_to_all x1, waiting for transfers between devices, sites_work(): d_next = jax.lax.all_to_all(found_now, mesh_ax, 0, 0)  49.6 us
  transfers between devices with their start and end apart: 4, of which 3 were waited for; matrix products, arithmetic and copies ran while one was open for 12% of the time, Pallas kernels for 0%

profile of v1, /device:TPU:0, one launch (start us, length us, event | category | flops | bytes accessed | tf_op | source)
XLA Modules:
  0.0 662.1 jit_solution(16060458931885874294)
XLA Ops:
  8.6 1.3 fusion.31
  9.9 1.2 fusion.33
  14.7 90.2 %all-gather.3.cloned.1.call-done = bf16[16384,320]{1,0:T(8,128)(2,1)} async-done(((bf16[1024,320]{1,0:T(8,128)(2,1)}), bf16[16384,320]{1,0:T(8,128)(2,1)}) %all-gather.3.cloned.1.call-update) | async-done | bytes 10485776 | tf_op jit(solution)/shard_map/all_gather | solution.py:16
  104.9 3.7 slice.39
  108.6 4.8 copy.29
  113.4 7.1 %slice.38 = bf16[16384,256]{1,0:T(8,128)(2,1)} slice(bf16[16384,320]{1,0:T(8,128)(2,1)} %all-gather.3.cloned.1.call-done), slice={[0:16384], [0:256]} | slice | bytes 16777216 | tf_op jit(solution)/shard_map/slice | solution.py:18
  122.6 57.8 %while.15 = (s32[]{:T(128)}, f32[2,1024]{1,0:T(2,128)S(1)}, f32[2,1024]{1,0:T(2,128)}, f32[2,1024,128]{2,1,0:T(8,128)}, s32[8]{0:T(128)}, /*index=5*/s32[]{:T(12...) while((s32[]{:T(128)}, f32[2,1024]{1,0:T(2,128)S(1)}, ...), condition=%wide.region_6.7_spmd.clone, body=%wide.region_1.6_spmd.clone.sunk | while | flops 3266845696 | bytes 178161584 | solution.py:109
  124.4 43.7 %conditional.3 = ((f32[2,1024]{1,0:T(2,128)S(1)}, f32[2,1024]{1,0:T(2,128)}, f32[2,1024,128]{2,1,0:T(8,128)})) conditional(s32[]{:T(128)} %convert_element_type.126, (f32[2,1024]{1,0:T(2,128)S(1)}, f32[2,1024]{1,0:T(2,128)}, f32[2,1024,128]{2,1,0:T(8,128)}) %tuple.44, (s32[]{:T(128)}, s32[]{:T(128)}, bf16[8,2048,256]{2,1,0:T(8,128)(2,1)}, s32[]{:T(128)}, ...), branch_computations={%region_2.2_spmd, %region_3.5_spmd} | conditional | flops 3266845696 | bytes 178157184 | solution.py:107
  124.4 1.8 convolution_convert_fusion.1
  126.1 8.1 %fusion.37 = f32[2,2048,1024]{2,1,0:T(8,128)} fusion(bf16[2048,2,128]{0,2,1:T(8,128)(2,1)S(1)} %bitcast.43, bf16[1024,2,128]{2,0,1:T(8,128)(2,1)S(1)} %get-tuple-element.152), kind=kOutput, calls=%fused_computation.62 | convolution fusion | flops 1073741824 | bytes 18350080 | tf_op jit(solution)/shard_map/while/body/eval_jaxpr/cond/branch_1_fun/qhd,khd->hqk/dot_general | solution.py:66
  134.3 1.3 broadcast_compare_fusion
  135.6 12.3 %fusion.36 = (f32[2,1024]{1,0:T(2,128)S(1)}, f32[2,1024,2048]{1,2,0:T(8,128)}) fusion(bf16[1024,2,64]{0,2,1:T(8,128)(2,1)} %get-tuple-element.154, bf16[8,2048,64]{1,2,0:T(8,128)(2,1)} %get-tuple-element.153, s32[]{:T(128)} %get-tuple-element.150, f32[2,2048,1024]{2,1,0:T(8,128)} %fusion.37, pred[1024,2048]{0,1:T(8,128)(4,1)S(1)} %broadcast_compare_fusion), kind=kOutput, calls=%fused_computation.61 | convolution fusion | flops 553646080 | bytes 36184576 | tf_op jit(solution)/shard_map/while/body/eval_jaxpr/cond/branch_1_fun/qhr,kr->hqk/dot_general | solution.py:67
  148.0 8.6 %fusion.5 = f32[2,1024]{1,0:T(2,128)S(1)} fusion(f32[2,1024,2048]{1,2,0:T(8,128)} %get-tuple-element.256, f32[2,1024]{1,0:T(2,128)S(1)} %max.4, pred[1024,2048]{0,1:T(8,128)(4,1)} %copy-done.2), kind=kLoop, calls=%fused_computation.6 | loop fusion | flops 12580864 | bytes 18890752 | tf_op jit(solution)/shard_map/while/body/eval_jaxpr/cond/branch_1_fun/reduce_sum | solution.py:74
  156.6 2.0 multiply_add_fusion
  158.6 1.8 convolution_convert_fusion
  160.4 7.7 %fusion.9 = f32[2,1024,128]{2,1,0:T(8,128)} fusion(bf16[2048,2,128]{0,2,1:T(8,128)(2,1)S(1)} %bitcast.45, f32[2,1024,2048]{1,2,0:T(8,128)S(1)} %copy-done.1, f32[2,1024]{1,0:T(2,128)S(1)} %max.4, pred[1024,2048]{0,1:T(8,128)(4,1)} %copy-done.2, f32[2,1024,128]{2,1,0:T(8,128)} %get-tuple-element.156, f32[2,1024]{1,0:T(2,128)S(1)} %get-tuple-element.254), kind=kOutput, calls=%fused_computation.12 | convolution fusion | flops 1086849024 | bytes 22036480 | tf_op jit(solution)/shard_map/while/body/eval_jaxpr/cond/branch_1_fun/hqk,khd->hqd/dot_general | solution.py:75
  168.1 1.1 dynamic_slice.38
  169.8 1.2 dynamic_slice.38
  171.6 1.2 dynamic_slice.38
  173.4 1.2 dynamic_slice.38
  175.1 1.2 dynamic_slice.38
  176.9 1.2 dynamic_slice.38
  178.7 1.2 dynamic_slice.38
  180.4 2.5 bitcast_convert_fusion
  183.0 53.7 %all_to_all.10 = bf16[8,128,2048]{2,1,0:T(8,128)(2,1)S(1)} all-to-all(bf16[8,128,2048]{2,1,0:T(8,128)(2,1)S(1)} %bitcast.47), channel_id=1, replica_groups=mesh['sp'=16,'tp'=8] {'tp'}, dimensions={0} | all-to-all | bytes 8388608 | tf_op jit(solution)/shard_map/all_to_all | solution.py:31
  238.2 2.5 stack.2
  240.7 4.6 all-to-all-start.1
  245.3 49.6 %all-to-all-done.1 = bf16[8,128,2048]{2,1,0:T(8,128)(2,1)} async-done(((bf16[8,128,2048]{2,1,0:T(8,128)(2,1)}), bf16[8,128,2048]{2,1,0:T(8,128)(2,1)}, u32[]{:S(2)}, u32[]{:S(2)}) %all-to-all-start.1) | async-done | bytes 4194336 | tf_op jit(solution)/shard_map/all_to_all | solution.py:191
  294.9 7.9 %fusion.25 = f32[1024,704]{0,1:T(8,128)} fusion(bf16[1024,2048]{1,0:T(8,128)(2,1)} %bitcast.14, bf16[2048,2112]{0,1:T(8,128)(2,1)} %all-gather.5.cloned.1.call-done), kind=kOutput, calls=%fused_computation.33 | convolution fusion | flops 2952790016 | bytes 9961472 | tf_op jit(solution)/shard_map/dot_general | solution.py:195
  302.8 12.0 %convolution_convert_fusion.2 = bf16[1024,2048]{1,0:T(8,128)(2,1)} fusion(bf16[2048,2112]{0,1:T(8,128)(2,1)} %all-gather.5.cloned.1.call-done, f32[1024,704]{0,1:T(8,128)} %fusion.25, bf16[1024,2048]{1,0:T(8,128)(2,1)} %bitcast.14), kind=kOutput, calls=%fused_computation.29 | convolution fusion | flops 5912002560 | bytes 17039360 | tf_op jit(solution)/shard_map/dot_general | solution.py:199
  314.8 338.7 %reduce-scatter.2.cloned.1.call-done = bf16[128,2048]{1,0:T(8,128)(2,1)} async-done(((bf16[1024,2048]{1,0:T(8,128)(2,1)}), bf16[128,2048]{1,0:T(8,128)(2,1)}) %reduce-scatter.2.cloned.1.call-update) | async-done | bytes 524304 | tf_op jit(solution)/shard_map/reduce_scatter | solution.py:202
  653.6 2.0 add_convert_fusion
  (71 shorter events, 10.4 us)
Async XLA Ops:
  6.5 173.9 %copy-start = (bf16[256,2048]{1,0:T(8,128)(2,1)S(1)}, bf16[256,2048]{1,0:T(8,128)(2,1)}, u32[]{:S(2)}) copy-start(bf16[256,2048]{1,0:T(8,128)(2,1)} %param.25) | copy-start | bytes 3145732
  6.5 5.8 copy-start.9
  6.5 5.8 copy-start.8
  6.5 5.8 copy-start.7
  6.5 6.7 %copy-start.6 = (bf16[1024,128]{1,0:T(8,128)(2,1)S(1)}, bf16[1024,128]{1,0:T(8,128)(2,1)}, u32[]{:S(2)}) copy-start(bf16[1024,128]{1,0:T(8,128)(2,1)} %param.19) | copy-start | bytes 786436
  6.5 6.9 %copy-start.5 = (bf16[1024,256]{1,0:T(8,128)(2,1)S(1)}, bf16[1024,256]{1,0:T(8,128)(2,1)}, u32[]{:S(2)}) copy-start(bf16[1024,256]{1,0:T(8,128)(2,1)} %param.18) | copy-start | bytes 1572868
  6.6 98.3 %all-gather.3.cloned.1.call-start = ((), (), s32[]{:S(2)}) async-start(), calls=%async_computation.3 | async-start | bytes 13369344 | tf_op jit(solution)/shard_map/all_gather | solution.py:16
  12.3 233.0 %all-gather.5.cloned.1.call-start = ((), (), s32[]{:S(2)}) async-start(), calls=%async_computation.4 | async-start | bytes 9191424 | tf_op jit(solution)/shard_map/all_gather | solution.py:16
  135.6 12.3 %copy-start.2 = (pred[1024,2048]{0,1:T(8,128)(4,1)}, pred[1024,2048]{0,1:T(8,128)(4,1)S(1)}, u32[]{:S(2)}) copy-start(pred[1024,2048]{0,1:T(8,128)(4,1)S(1)} %broadcast_compare_fusion) | copy-start | bytes 6291460 | tf_op jit(solution)/shard_map/while/body/eval_jaxpr/cond
  147.9 10.7 %copy-start.4 = (bf16[256,256]{1,0:T(8,128)(2,1)S(1)}, bf16[256,256]{1,0:T(8,128)(2,1)}, u32[]{:S(2)}) copy-start(bf16[256,256]{1,0:T(8,128)(2,1)} %get-tuple-element.157) | copy-start | bytes 393220 | tf_op jit(solution)/shard_map/while/body/eval_jaxpr/cond
  147.9 12.4 %copy-start.1 = (f32[2,1024,2048]{1,2,0:T(8,128)S(1)}, f32[2,1024,2048]{1,2,0:T(8,128)}, u32[]{:S(2)}) copy-start(f32[2,1024,2048]{1,2,0:T(8,128)} %get-tuple-element.256) | copy-start | bytes 50331652 | tf_op jit(solution)/shard_map/while/body/eval_jaxpr/cond
  236.7 1.0 copy-start.3
  236.7 1.3 copy-start.10
  240.7 54.2 %all-to-all-start.1 = ((bf16[8,128,2048]{2,1,0:T(8,128)(2,1)}), bf16[8,128,2048]{2,1,0:T(8,128)(2,1)}, u32[]{:S(2)}, u32[]{:S(2)}) async-start(bf16[8,128,2048]{2,1,0:T(8,128)(2,1)} %stack.2), calls=%async_computation.1 | async-start | bytes 8388608 | tf_op jit(solution)/shard_map/all_to_all | solution.py:191
  245.3 408.3 %reduce-scatter.2.cloned.1.call-start = ((), (), s32[]{:S(2)}) async-start(), calls=%async_computation.5 | async-start | bytes 4718592 | tf_op jit(solution)/shard_map/reduce_scatter | solution.py:202
Sparse Core Ops, SparseCore 0:
  12.4 92.3 all-gather.2
  107.0 78.2 all-gather.4
  315.0 338.5 reduce-scatter.1
